TPU v7x, 32 devices: a whole 2x2x4 slice. The times are simulated.
32 devices in a mesh: ep: 8 (over z, x), tp: 4 (over y, core).
Axes of the slice: x: 2, y: 2, z: 4, core: 2. Of those that a mesh axis runs over, the one named last changes fastest.
Arguments:
- residual_in: bfloat16 [128, 2048], P('ep'), may hold values from -6 to 6
- lengths: int32 [128], P('ep'), may hold values from 1 to 511, as said below
- kv_cache: bfloat16 [128, 4, 512, 256], P('ep', 'tp'), may hold values from -640 to 640
- norm_gain_attn: float32 [2048], replicated, may hold values from 0.1 to 1.9
- query_weight: bfloat16 [2048, 2048], P(None, 'tp'), may hold values from -0.125 to 0.125
- key_weight: bfloat16 [2048, 512], P(None, 'tp'), may hold values from -0.125 to 0.125
- value_weight: bfloat16 [2048, 512], P(None, 'tp'), may hold values from -0.125 to 0.125
- diff_lambda: float32 [16], P('tp'), may hold values from 0.3 to 0.8
- head_gain: float32 [128], replicated, may hold values from 0.1 to 1.9
- out_weight: bfloat16 [2048, 2048], P(None, 'tp'), may hold values from -0.125 to 0.125
- norm_gain_ffn: float32 [2048], replicated, may hold values from 0.1 to 1.9
- route_ids: int32 [128, 2], P('ep'), may hold values from 0 to 7, as said below
- route_weights: float32 [128, 2], P('ep'), may hold values from 0.1 to 1
- expert_gate: bfloat16 [8, 2048, 512], P('ep', None, 'tp'), may hold values from -0.125 to 0.125
- expert_up: bfloat16 [8, 2048, 512], P('ep', None, 'tp'), may hold values from -0.125 to 0.125
- expert_down: bfloat16 [8, 512, 2048], P('ep', 'tp'), may hold values from -0.25 to 0.25
- dense_gate: bfloat16 [2048, 8192], P(None, 'ep'), may hold values from -0.125 to 0.125
- dense_up: bfloat16 [2048, 8192], P(None, 'ep'), may hold values from -0.125 to 0.125
- dense_down: bfloat16 [8192, 2048], P('ep'), may hold values from -0.0625 to 0.0625
- dense_mix: float32 [2048], replicated, may hold values from -0.125 to 0.125
Outputs:
- layer_out: bfloat16 [128, 2048], P('ep', 'tp')
- new_rows: bfloat16 [128, 4, 256], P('ep', 'tp')
Inputs may be any that keep to these rules, and one draw needn't show every extreme that they name: The new token stands at position lengths[b]; some sequence holds 511 positions in every draw. `route_ids`: each row names 2 different experts from one group; the groups are the 4 runs of consecutive expert numbers of equal size. Among the rows of one index of ep no expert is named more than 8 times, and some expert exactly 8 times.
All inputs are finite; a program needn't handle non-finite values.
Results may differ from a plain program's by a relative error of at most 0.008.
The roundings to bfloat16 on the way count: a program that leaves them out, or rounds other values in their place, can miss the bound.
Values may be sent and summed in bfloat16 or wider, within the bound.
A program may use at most 64 MiB of HBM per device.

v0:
```python
import jax
import jax.numpy as jnp
from jax import lax
from jax.sharding import PartitionSpec as P

QK_DIM = 64
HEAD_DIM = 128
TOPK = 2
EPS = 1e-06


def rms_rows(values, gain):
    mean_sq = jnp.mean(values * values, axis=-1, keepdims=True)
    return values * lax.rsqrt(mean_sq + EPS) * gain


def rotate(vectors, positions):
    half = vectors.shape[-1] // 2
    inverse = 10000.0 ** (-jnp.arange(half, dtype=jnp.float32) / half)
    angle = positions[:, None, None, None] * inverse
    cosine = jnp.cos(angle)
    sine = jnp.sin(angle)
    first = vectors[..., :half]
    second = vectors[..., half:]
    return jnp.concatenate(
        [first * cosine - second * sine, first * sine + second * cosine], axis=-1
    )


def normalize(scores, latest, valid):
    masked = jnp.where(valid, scores, -jnp.inf)
    top = jnp.maximum(jnp.max(masked, axis=-1), latest)
    raised = jnp.where(valid, jnp.exp(jnp.where(valid, scores, 0.0) - top[..., None]), 0.0)
    raised_new = jnp.exp(latest - top)
    total = jnp.sum(raised, axis=-1) + raised_new
    return (raised / total[..., None], raised_new / total)


def attend(query, fresh, cache, lengths, lam):
    count = fresh.shape[0]
    groups = fresh.shape[1]
    share = query.shape[1] // groups
    scale = QK_DIM ** (-0.5)
    grouped = query.reshape(count, groups, share, 2, QK_DIM)
    first = (
        jnp.einsum(
            "bgjd,bgkd->bgjk",
            grouped[:, :, :, 0],
            cache[..., :QK_DIM],
            preferred_element_type=jnp.float32,
        )
        * scale
    )
    second = (
        jnp.einsum(
            "bgjd,bgkd->bgjk",
            grouped[:, :, :, 1],
            cache[..., QK_DIM : 2 * QK_DIM],
            preferred_element_type=jnp.float32,
        )
        * scale
    )
    first_new = (
        jnp.einsum(
            "bgjd,bgd->bgj",
            grouped[:, :, :, 0],
            fresh[..., :QK_DIM],
            preferred_element_type=jnp.float32,
        )
        * scale
    )
    second_new = (
        jnp.einsum(
            "bgjd,bgd->bgj",
            grouped[:, :, :, 1],
            fresh[..., QK_DIM : 2 * QK_DIM],
            preferred_element_type=jnp.float32,
        )
        * scale
    )
    valid = (
        jnp.arange(cache.shape[2], dtype=jnp.int32)[None, None, None, :]
        < lengths[:, None, None, None]
    )
    prob_one, prob_one_new = normalize(first, first_new, valid)
    prob_two, prob_two_new = normalize(second, second_new, valid)
    weight = lam.reshape(groups, share)[None, :, :, None]
    mapped = (prob_one - weight * prob_two).astype(jnp.bfloat16)
    mapped_new = (prob_one_new - weight[..., 0] * prob_two_new).astype(jnp.bfloat16)
    output = jnp.einsum(
        "bgjk,bgkd->bgjd", mapped, cache[..., 2 * QK_DIM :], preferred_element_type=jnp.float32
    )
    output = output + mapped_new.astype(jnp.float32)[..., None] * fresh[
        :, :, None, 2 * QK_DIM :
    ].astype(jnp.float32)
    return output.reshape(count, groups * share, HEAD_DIM)


def on_device(
    residual_in,
    lengths,
    kv_cache,
    norm_gain_attn,
    query_weight,
    key_weight,
    value_weight,
    diff_lambda,
    head_gain,
    out_weight,
    norm_gain_ffn,
    route_ids,
    route_weights,
    expert_gate,
    expert_up,
    expert_down,
    dense_gate,
    dense_up,
    dense_down,
    dense_mix,
):
    seq_count, width = residual_in.shape
    lanes = lax.axis_size("tp")
    column = lax.axis_index("tp")
    quarter = width // lanes
    groups = kv_cache.shape[1]
    local_heads = diff_lambda.shape[0]
    resid = residual_in.astype(jnp.float32)
    normed = rms_rows(resid, norm_gain_attn).astype(jnp.bfloat16)
    positions = lengths.astype(jnp.float32)
    query = jnp.dot(normed, query_weight, preferred_element_type=jnp.float32).reshape(
        seq_count, local_heads, 2, QK_DIM
    )
    query = rotate(query, positions).astype(jnp.bfloat16)
    keys = jnp.dot(normed, key_weight, preferred_element_type=jnp.float32).reshape(
        seq_count, groups, 2, QK_DIM
    )
    keys = rotate(keys, positions).astype(jnp.bfloat16).reshape(seq_count, groups, 2 * QK_DIM)
    values = (
        jnp.dot(normed, value_weight, preferred_element_type=jnp.float32)
        .reshape(seq_count, groups, HEAD_DIM)
        .astype(jnp.bfloat16)
    )
    fresh = jnp.concatenate([keys, values], axis=-1)
    mixed = attend(query, fresh, kv_cache, lengths, diff_lambda)
    heads_out = (
        rms_rows(mixed, head_gain).astype(jnp.bfloat16).reshape(seq_count, local_heads * HEAD_DIM)
    )
    all_heads = lax.all_gather(heads_out, "tp", axis=1, tiled=True)
    attn_cols = jnp.dot(all_heads, out_weight, preferred_element_type=jnp.float32)
    own_cols = lax.dynamic_slice_in_dim(resid, column * quarter, quarter, 1)
    stream_cols = (own_cols + attn_cols).astype(jnp.bfloat16)
    stream = lax.all_gather(stream_cols, "tp", axis=1, tiled=True)
    ffn_in = rms_rows(stream.astype(jnp.float32), norm_gain_ffn).astype(jnp.bfloat16)
    held = expert_gate.shape[0]
    expert_total = lax.axis_size("ep") * held
    capacity = max(2, 2 * TOPK * seq_count // expert_total)
    flat_ids = route_ids.reshape(-1)
    member = (flat_ids[:, None] == jnp.arange(expert_total, dtype=jnp.int32)[None, :]).astype(
        jnp.int32
    )
    slot = jnp.sum((jnp.cumsum(member, axis=0) - member) * member, axis=1)
    target = (flat_ids * capacity + slot).reshape(seq_count, TOPK)
    picker = (
        target[None, :, :] == jnp.arange(expert_total * capacity, dtype=jnp.int32)[:, None, None]
    )
    picker = jnp.any(picker, axis=2).astype(jnp.bfloat16)
    outgoing = jnp.dot(picker, ffn_in, preferred_element_type=jnp.float32).astype(jnp.bfloat16)
    outgoing = outgoing.reshape(expert_total, capacity, ffn_in.shape[1])
    arrived = lax.all_to_all(outgoing, "ep", split_axis=0, concat_axis=0, tiled=True)
    senders = arrived.shape[0] // held
    blocked = arrived.reshape(senders, held, arrived.shape[1], width)
    gate = jnp.einsum("sjcd,jdf->sjcf", blocked, expert_gate, preferred_element_type=jnp.float32)
    upward = jnp.einsum("sjcd,jdf->sjcf", blocked, expert_up, preferred_element_type=jnp.float32)
    hidden = (jax.nn.silu(gate) * upward).astype(jnp.bfloat16)
    partial_out = jnp.einsum(
        "sjcf,jfd->sjcd", hidden, expert_down, preferred_element_type=jnp.float32
    )
    partial_out = partial_out.reshape(arrived.shape[0], arrived.shape[1], width)
    summed = lax.psum_scatter(
        partial_out.astype(jnp.bfloat16), "tp", scatter_dimension=2, tiled=True
    )
    returned = lax.all_to_all(summed, "ep", split_axis=0, concat_axis=0, tiled=True)
    flat_back = returned.reshape(expert_total * capacity, quarter)
    picked = flat_back[target]
    expert_cols = jnp.sum(route_weights[..., None] * picked.astype(jnp.float32), axis=1)
    gate_mix = jax.nn.sigmoid(jnp.sum(ffn_in.astype(jnp.float32) * dense_mix, axis=-1))
    share_rows = seq_count // lanes
    mine = lax.dynamic_slice_in_dim(ffn_in, column * share_rows, share_rows, 0)
    piece = lax.all_gather(mine, "ep", axis=0, tiled=True)
    gate = jnp.dot(piece, dense_gate, preferred_element_type=jnp.float32)
    upward = jnp.dot(piece, dense_up, preferred_element_type=jnp.float32)
    dense_hidden = (jax.nn.silu(gate) * upward).astype(jnp.bfloat16)
    dense_cols = lax.psum_scatter(
        jnp.dot(dense_hidden, dense_down, preferred_element_type=jnp.float32),
        "ep",
        scatter_dimension=0,
        tiled=True,
    )
    dense_cols = lax.all_to_all(
        dense_cols.astype(jnp.bfloat16), "tp", split_axis=1, concat_axis=0, tiled=True
    ).astype(dense_cols.dtype)
    layer_out = (
        stream_cols.astype(jnp.float32) + expert_cols + gate_mix[:, None] * dense_cols
    ).astype(jnp.bfloat16)
    return (layer_out, fresh)


def solution(mesh):
    placed = (
        P("ep", None),
        P("ep"),
        P("ep", "tp", None, None),
        P(),
        P(None, "tp"),
        P(None, "tp"),
        P(None, "tp"),
        P("tp"),
        P(),
        P(None, "tp"),
        P(),
        P("ep", None),
        P("ep", None),
        P("ep", None, "tp"),
        P("ep", None, "tp"),
        P("ep", "tp", None),
        P(None, "ep"),
        P(None, "ep"),
        P("ep", None),
        P(),
    )
    return jax.shard_map(
        on_device,
        mesh=mesh,
        in_specs=placed,
        out_specs=(P("ep", "tp"), P("ep", "tp", None)),
        check_vma=False,
    )
```

profile of v0, /device:TPU:0, one launch (start us, length us, event | category | flops | bytes accessed | tf_op | source)
XLA Modules:
  0.0 165.9 jit_solution(6346756929134641032)
XLA Ops:
  7.2 0.0 copy-start
  7.2 0.8 convert_element_type.109
  8.0 0.7 iota_compare_fusion
  8.7 1.0 multiply_reduce_fusion.1
  9.7 0.9 convert_element_type.107
  10.6 1.3 fusion.73
  11.9 1.3 fusion.70
  13.2 0.1 reshape.337
  13.3 0.1 fusion.72
  13.5 1.3 fusion.69
  14.8 0.1 reshape.340
  14.9 0.1 multiply_cosine_fusion
  15.0 0.1 subtract_convert_fusion.1
  15.1 0.1 pad_maximum_fusion.1
  15.2 0.1 convert_element_type.110
  15.3 0.1 slice_bitcast_fusion.4
  15.4 0.1 fusion.55
  15.5 0.1 fusion.59
  15.6 2.5 %fusion.11 = f32[16,4,512]{2,1,0:T(4,128)S(1)} fusion(bf16[16,4,64]{2,1,0:T(4,128)(2,1)S(1)} %get-tuple-element.12, bf16[16,1,512,256]{3,2,1,0:T(8,128)(2,1)} %param.22), kind=kOutput, calls=%fused_computation.14 | convolution fusion | flops 4227072 | bytes 2236416 | tf_op jit(solution)/shard_map/bgjd,bgkd->bgjk/dot_general | solution.py:55
  18.2 0.1 fusion.61
  18.3 2.3 %select_reduce_fusion.1 = (f32[16,4]{1,0:T(8,128)S(1)}, f32[16,4]{1,0:T(8,128)S(1)}, f32[16,4,512]{2,1,0:T(4,128)S(1)}) fusion(pred[16,512]{1,0:T(8,128)(4,1)S(1)} %iota_compare_fusion, f32[16,4,512]{2,1,0:T(4,128)S(1)} %fusion.11, bf16[16,4,64]{2,1,0:T(4,128)(2,1)S(1)} %get-tuple-element.13, bf16[16,1,512,256]{3,2,1,0:T(8,128)(2,1)} %param.22), kind=kOutput, calls=%fused_computation.44 | convolution fusion | flops 4358016 | bytes 2376192 | tf_op jit(solution)/shard_map/bgjd,bgkd->bgjk/dot_general | solution.py:46
  20.6 0.0 copy-start.4
  20.7 0.3 fusion.34
  21.0 0.6 multiply_reduce_fusion.3
  21.6 0.1 broadcast_multiply_fusion
  21.7 6.2 %all_gather.9 = bf16[16,2048]{1,0:T(8,128)(2,1)S(1)} all-gather(bf16[16,512]{1,0:T(8,128)(2,1)S(1)} %fusion.45), channel_id=1, replica_groups=mesh['ep'=8,'tp'=4] {'tp'}, dimensions={1}, use_global_device_ids=true | all-gather | bytes 81920 | tf_op jit(solution)/shard_map/all_gather | solution.py:148
  28.0 2.0 %fusion.18 = bf16[16,512]{1,0:T(8,128)(2,1)S(1)} fusion(bf16[16,2048]{1,0:T(8,128)(2,1)S(1)} %all_gather.9, bf16[2048,512]{1,0:T(8,128)(2,1)} %param.29, f32[16,2048]{1,0:T(8,128)S(1)} %convert_element_type.107, s32[]{:T(128)S(6)} %select_n.34), kind=kOutput, calls=%fused_computation.22 | convolution fusion | flops 33570816 | bytes 2211844 | tf_op jit(solution)/shard_map/dot_general | solution.py:149
  29.9 5.5 %all_gather.10 = bf16[16,2048]{1,0:T(8,128)(2,1)S(1)} all-gather(bf16[16,512]{1,0:T(8,128)(2,1)S(1)} %fusion.18), channel_id=1, replica_groups=mesh['ep'=8,'tp'=4] {'tp'}, dimensions={1}, use_global_device_ids=true | all-gather | bytes 81920 | tf_op jit(solution)/shard_map/all_gather | solution.py:152
  35.5 0.1 fusion.25
  35.6 0.1 copy.69
  35.7 0.1 eq.28
  35.8 0.1 fusion.57
  35.9 0.1 reduce_window_sum.11
  35.9 0.2 select_reduce_fusion.2
  36.1 0.1 reduce_sum.79
  36.2 0.1 copy.70
  36.3 0.1 fusion.58
  36.4 0.0 copy-done.4
  36.4 0.2 multiply_reduce_fusion
  36.6 1.0 fusion
  37.6 6.0 %all-to-all-start = ((bf16[8,8,2048]{2,1,0:T(8,128)(2,1)}), bf16[8,8,2048]{2,1,0:T(8,128)(2,1)S(1)}, u32[]{:S(2)}, u32[]{:S(2)}) async-start(bf16[8,8,2048]{2,1,0:T(8,128)(2,1)} %fusion), calls=%async_computation | async-start | bytes 524288 | tf_op jit(solution)/shard_map/all_to_all | solution.py:169
  43.5 0.0 reduce-scatter.2.cloned.1.call-start
  43.6 33.4 %all-gather = bf16[8,4,2048]{2,1,0:T(4,128)(2,1)S(1)} all-gather(bf16[1,4,2048]{2,1,0:T(4,128)(2,1)S(1)} %dynamic-slice_bitcast_fusion), channel_id=1, replica_groups=mesh['ep'=8,'tp'=4] {'ep'}, dimensions={0}, use_global_device_ids=true | all-gather | bytes 147456 | tf_op jit(solution)/shard_map/all_gather | solution.py:189
  77.1 3.0 %fusion.74 = f32[32,1024]{1,0:T(8,128)S(1)} fusion(bf16[32,2048]{1,0:T(8,128)(2,1)S(1)} %reshape.365, bf16[2048,1024]{1,0:T(8,128)(2,1)} %param.36), kind=kOutput, calls=%fused_computation.125 | convolution fusion | flops 134217728 | bytes 4456448 | tf_op jit(solution)/shard_map/dot_general | solution.py:190
  80.1 0.0 copy-start.2
  80.1 5.1 %fusion.15 = f32[32,2048]{1,0:T(8,128)S(1)} fusion(bf16[1024,2048]{1,0:T(8,128)(2,1)} %param.38, bf16[32,2048]{1,0:T(8,128)(2,1)S(1)} %reshape.365, bf16[2048,1024]{1,0:T(8,128)(2,1)} %param.37, f32[32,1024]{1,0:T(8,128)S(1)} %fusion.74), kind=kOutput, calls=%fused_computation.16 | convolution fusion | flops 268632064 | bytes 8912896 | tf_op jit(solution)/shard_map/dot_general | solution.py:194
  85.2 0.6 dynamic-slice
  86.4 37.8 %all-reduce.2 = bf16[32,2048]{1,0:T(8,128)(2,1)S(1)} all-reduce(f32[32,2048]{1,0:T(8,128)S(1)} %fusion.15), channel_id=3, replica_groups=mesh['ep'=8,'tp'=4] {'ep'}, use_global_device_ids=true, to_apply=%region_13.14.clone | all-reduce | flops 65536 | bytes 393216
  124.2 1.3 convolution_bitcast_fusion.1
  125.5 2.1 %convolution_convert_fusion = bf16[8,8,2048]{2,1,0:T(8,128)(2,1)} fusion(bf16[8,8,2048]{2,1,0:T(8,128)(2,1)S(1)} %all-to-all-done, bf16[1,128,2048]{2,1,0:T(8,128)(2,1)S(1)} %copy-done.2, bf16[1,2048,128]{2,1,0:T(8,128)(2,1)} %param.34, f32[8,1,8,128]{3,2,0,1:T(8,128)S(1)} %convolution_bitcast_fusion.1), kind=kOutput, calls=%fused_computation.1 | convolution fusion | flops 67289088 | bytes 1605632 | tf_op jit(solution)/shard_map/sjcf,jfd->sjcd/dot_general | solution.py:175
  127.6 0.0 reduce-scatter.2.cloned.1.call-update
  127.6 0.6 dynamic-slice_convert_fusion
  128.3 3.3 %all-to-all-start.2 = ((bf16[4,4,512]{2,0,1:T(4,128)(2,1)}), bf16[4,4,512]{2,0,1:T(4,128)(2,1)S(1)}, u32[]{:S(2)}, u32[]{:S(2)}) async-start(bf16[4,4,512]{2,0,1:T(4,128)(2,1)} %bitcast.35), calls=%async_computation.3 | async-start | bytes 32768 | tf_op jit(solution)/shard_map/all_to_all | solution.py:199
  131.5 0.1 copy.71
  131.6 0.1 reshape.355
  131.7 0.6 pad_maximum_fusion.2
  132.3 0.1 copy.68
  132.4 2.9 %all-to-all-done.2 = bf16[4,4,512]{2,0,1:T(4,128)(2,1)S(1)} async-done(((bf16[4,4,512]{2,0,1:T(4,128)(2,1)}), bf16[4,4,512]{2,0,1:T(4,128)(2,1)S(1)}, u32[]{:S(2)}, u32[]{:S(2)}) %all-to-all-start.2) | async-done | bytes 16416 | tf_op jit(solution)/shard_map/all_to_all | solution.py:199
  135.4 9.8 %reduce-scatter.2.cloned.1.call-done = bf16[8,8,512]{2,1,0:T(8,128)(2,1)} async-done(((bf16[8,8,2048]{2,1,0:T(8,128)(2,1)}), bf16[8,8,512]{2,1,0:T(8,128)(2,1)}) %reduce-scatter.2.cloned.1.call-update) | async-done | bytes 65552 | tf_op jit(solution)/shard_map/reduce_scatter | solution.py:179
  145.2 5.5 %all-to-all-start.1 = ((bf16[8,8,512]{2,1,0:T(8,128)(2,1)}), bf16[8,8,512]{2,1,0:T(8,128)(2,1)S(1)}, u32[]{:S(2)}, u32[]{:S(2)}) async-start(bf16[8,8,512]{2,1,0:T(8,128)(2,1)} %reduce-scatter.2.cloned.1.call-done), calls=%async_computation.2 | async-start | bytes 131072 | tf_op jit(solution)/shard_map/all_to_all | solution.py:182
  150.7 6.9 %all-to-all-done.1 = bf16[8,8,512]{2,1,0:T(8,128)(2,1)S(1)} async-done(((bf16[8,8,512]{2,1,0:T(8,128)(2,1)}), bf16[8,8,512]{2,1,0:T(8,128)(2,1)S(1)}, u32[]{:S(2)}, u32[]{:S(2)}) %all-to-all-start.1) | async-done | bytes 65568 | tf_op jit(solution)/shard_map/all_to_all | solution.py:182
  157.6 0.6 gather_fusion
  158.2 0.1 multiply_reduce_fusion.2
  158.4 0.7 add_convert_fusion.1
  (34 shorter events, 0.3 us)
Async XLA Ops:
  7.2 4.7 %copy-start = (bf16[2048,512]{1,0:T(8,128)(2,1)S(1)}, bf16[2048,512]{1,0:T(8,128)(2,1)}, u32[]{:S(2)}) copy-start(bf16[2048,512]{1,0:T(8,128)(2,1)} %param.24) | copy-start | bytes 6291460
  11.9 9.1 %copy-start.7 = (f32[4]{0:T(128)S(1)}, f32[4]{0:T(128)}, u32[]{:S(2)}) copy-start(f32[4]{0:T(128)} %param.27) | copy-start | bytes 52
  15.3 5.7 %copy-start.1 = (bf16[16,1,512,256]{3,2,1,0:T(8,128)(2,1)S(1)}, bf16[16,1,512,256]{3,2,1,0:T(8,128)(2,1)}, u32[]{:S(2)}) copy-start(bf16[16,1,512,256]{3,2,1,0:T(8,128)(2,1)} %param.22) | copy-start | bytes 12582916
  18.2 3.5 %copy-start.8 = (f32[128]{0:T(128)S(1)}, f32[128]{0:T(128)}, u32[]{:S(2)}) copy-start(f32[128]{0:T(128)} %param.28) | copy-start | bytes 1540
  20.6 15.0 %copy-start.5 = (s32[16,2]{0,1:T(2,128)S(1)}, s32[16,2]{0,1:T(2,128)}, u32[]{:S(2)}) copy-start(s32[16,2]{0,1:T(2,128)} %param.31) | copy-start | bytes 388
  20.6 15.7 %copy-start.3 = (f32[2048]{0:T(1024)S(1)}, f32[2048]{0:T(1024)}, u32[]{:S(2)}) copy-start(f32[2048]{0:T(1024)} %param.39) | copy-start | bytes 24580
  20.6 15.7 %copy-start.4 = (f32[2048]{0:T(1024)S(1)}, f32[2048]{0:T(1024)}, u32[]{:S(2)}) copy-start(f32[2048]{0:T(1024)} %param.30) | copy-start | bytes 24580
  37.6 86.6 %all-to-all-start = ((bf16[8,8,2048]{2,1,0:T(8,128)(2,1)}), bf16[8,8,2048]{2,1,0:T(8,128)(2,1)S(1)}, u32[]{:S(2)}, u32[]{:S(2)}) async-start(bf16[8,8,2048]{2,1,0:T(8,128)(2,1)} %fusion), calls=%async_computation | async-start | bytes 524288 | tf_op jit(solution)/shard_map/all_to_all | solution.py:169
  43.5 101.6 %reduce-scatter.2.cloned.1.call-start = ((), (), s32[]{:S(2)}) async-start(), calls=%async_computation.4 | async-start | bytes 327680 | tf_op jit(solution)/shard_map/reduce_scatter | solution.py:179
  80.1 5.1 %copy-start.9 = (u32[32]{0:T(128)S(1)}, u32[32]{0:T(128)}, u32[]{:S(2)}) copy-start(u32[32]{0:T(128)} %constant.59) | copy-start | bytes 388
  80.1 45.4 %copy-start.2 = (bf16[1,128,2048]{2,1,0:T(8,128)(2,1)S(1)}, bf16[1,128,2048]{2,1,0:T(8,128)(2,1)}, u32[]{:S(2)}) copy-start(bf16[1,128,2048]{2,1,0:T(8,128)(2,1)} %param.35) | copy-start | bytes 1572868
  80.1 52.2 %copy-start.6 = (f32[16,2]{0,1:T(2,128)S(1)}, f32[16,2]{0,1:T(2,128)}, u32[]{:S(2)}) copy-start(f32[16,2]{0,1:T(2,128)} %param.32) | copy-start | bytes 388
  128.3 7.1 %all-to-all-start.2 = ((bf16[4,4,512]{2,0,1:T(4,128)(2,1)}), bf16[4,4,512]{2,0,1:T(4,128)(2,1)S(1)}, u32[]{:S(2)}, u32[]{:S(2)}) async-start(bf16[4,4,512]{2,0,1:T(4,128)(2,1)} %bitcast.35), calls=%async_computation.3 | async-start | bytes 32768 | tf_op jit(solution)/shard_map/all_to_all | solution.py:199
  145.2 12.4 %all-to-all-start.1 = ((bf16[8,8,512]{2,1,0:T(8,128)(2,1)}), bf16[8,8,512]{2,1,0:T(8,128)(2,1)S(1)}, u32[]{:S(2)}, u32[]{:S(2)}) async-start(bf16[8,8,512]{2,1,0:T(8,128)(2,1)} %reduce-scatter.2.cloned.1.call-done), calls=%async_computation.2 | async-start | bytes 131072 | tf_op jit(solution)/shard_map/all_to_all | solution.py:182
Sparse Core Ops, SparseCore 0:
  127.8 17.3 reduce-scatter.1
where the time goes:
time: 167 us; the launch traced here: 166 us
  blocking collectives  82.9 us (50%)
  matrix products  24.1 us (14%)
  waiting for transfers between devices  19.6 us (12%)
  between operations  15 us (9%)
  starting transfers between devices  14.8 us (9%)
  other arithmetic  6.43 us (4%)
  local copies, waits for them, and re-layouts  3.1 us (2%)
    unnamed x1, blocking collectives  37.8 us
    all_gather x1, blocking collectives, on_device(): piece = lax.all_gather(mine, 'ep', axis=0, tiled=True)  33.4 us
    reduce_scatter x1, waiting for transfers between devices, on_device(): lax.psum_scatter(partial_out.astype(jnp.bfloat16), 'tp', scatter_dimensio...  9.79 us
    all_to_all x1, waiting for transfers between devices, on_device(): lax.all_to_all(summed, 'ep', split_axis=0, concat_axis=0, tiled=True)  6.88 us
    all_gather x1, blocking collectives, on_device(): all_heads = lax.all_gather(heads_out, 'tp', axis=1, tiled=True)  6.24 us
    all_to_all x1, starting transfers between devices, on_device(): lax.all_to_all(outgoing, 'ep', split_axis=0, concat_axis=0, tiled=True)  5.98 us
    all_gather x1, blocking collectives, on_device(): stream = lax.all_gather(stream_cols, 'tp', axis=1, tiled=True)  5.52 us
    all_to_all x1, starting transfers between devices, on_device(): lax.all_to_all(summed, 'ep', split_axis=0, concat_axis=0, tiled=True)  5.5 us
  transfers between devices with their start and end apart: 4, of which 3 were waited for; matrix products, arithmetic and copies ran while one was open for 6% of the time, Pallas kernels for 0%

commit v1 on v0

--- a/solution.py
+++ b/solution.py
@@ -186,7 +186,12 @@
     gate_mix = jax.nn.sigmoid(jnp.sum(ffn_in.astype(jnp.float32) * dense_mix, axis=-1))
     share_rows = seq_count // lanes
     mine = lax.dynamic_slice_in_dim(ffn_in, column * share_rows, share_rows, 0)
-    piece = lax.all_gather(mine, "ep", axis=0, tiled=True)
+    ring = [mine]
+    for hop in range(7):
+        ring.append(lax.ppermute(ring[-1], "ep", [(dev, (dev + 1) % 8) for dev in range(8)]))
+    piece = jnp.roll(
+        jnp.concatenate(ring[::-1], axis=0), (lax.axis_index("ep") + 1) * ring[0].shape[0], axis=0
+    )
     gate = jnp.dot(piece, dense_gate, preferred_element_type=jnp.float32)
     upward = jnp.dot(piece, dense_up, preferred_element_type=jnp.float32)
     dense_hidden = (jax.nn.silu(gate) * upward).astype(jnp.bfloat16)

time: 167 us -> 159 us (0.952)
  blocking collectives: 82.9 us -> 47.9 us
  waiting for transfers between devices: 19.6 us -> 45.2 us
  starting transfers between devices: 14.8 us -> 16.9 us
    ppermute x0 -> x7, waiting for transfers between devices: none -> 34.6 us  [on_device(): lax.ppermute(ring[-1], 'ep', [(dev, (dev + 1) % 8) for dev in range(8)])]
    all_gather x1 -> x0, blocking collectives: 33.4 us -> none  [on_device(): piece = lax.all_gather(mine, 'ep', axis=0, tiled=True)]
    reduce_scatter x1, waiting for transfers between devices: 9.79 us -> 0.01 us  [on_device(): lax.psum_scatter(partial_out.astype(jnp.bfloat16), 'tp', scatter_dimensio...]
    ppermute x0 -> x7, starting transfers between devices: none -> 3.77 us  [on_device(): lax.ppermute(ring[-1], 'ep', [(dev, (dev + 1) % 8) for dev in range(8)])]
  transfers between devices with their start and end apart: 4 -> 11, of which waited for: 3 -> 8; matrix products, arithmetic and copies ran while one was open for 6% -> 8% of each run, Pallas kernels for 0% -> 0%
where the time goes in v1:
time: 159 us; the launch traced here: 158 us
  blocking collectives  47.9 us (30%)
  waiting for transfers between devices  45.2 us (28%)
  matrix products  23 us (14%)
  starting transfers between devices  16.9 us (11%)
  between operations  15.1 us (9%)
  other arithmetic  6.42 us (4%)
  local copies, waits for them, and re-layouts  3.32 us (2%)
    unnamed x1, blocking collectives  36.2 us
    ppermute x7, waiting for transfers between devices, on_device(): lax.ppermute(ring[-1], 'ep', [(dev, (dev + 1) % 8) for dev in range(8)])  34.6 us
    all_to_all x1, waiting for transfers between devices, on_device(): lax.all_to_all(summed, 'ep', split_axis=0, concat_axis=0, tiled=True)  6.88 us
    all_gather x1, blocking collectives, on_device(): all_heads = lax.all_gather(heads_out, 'tp', axis=1, tiled=True)  6.24 us
    all_to_all x1, starting transfers between devices, on_device(): lax.all_to_all(outgoing, 'ep', split_axis=0, concat_axis=0, tiled=True)  6 us
    all_gather x1, blocking collectives, on_device(): stream = lax.all_gather(stream_cols, 'tp', axis=1, tiled=True)  5.52 us
    dot_general x1, matrix products, on_device(): jnp.dot(dense_hidden, dense_down, preferred_element_type=jnp.float32)  5.07 us
    all_to_all x1, starting transfers between devices, on_device(): lax.all_to_all(summed, 'ep', split_axis=0, concat_axis=0, tiled=True)  3.84 us
  transfers between devices with their start and end apart: 11, of which 8 were waited for; matrix products, arithmetic and copies ran while one was open for 8% of the time, Pallas kernels for 0%

profile of v1, /device:TPU:0, one launch (start us, length us, event | category | flops | bytes accessed | tf_op | source)
XLA Modules:
  0.0 157.8 jit_solution(13260649364960444226)
XLA Ops:
  7.2 0.8 convert_element_type.109
  8.0 0.7 iota_compare_fusion
  8.8 1.0 multiply_reduce_fusion.1
  9.7 0.9 convert_element_type.107
  10.6 1.3 fusion.75
  11.9 0.1 reshape.337
  12.0 0.1 fusion.77
  12.2 1.3 fusion.74
  13.5 0.1 reshape.340
  13.6 0.1 multiply_cosine_fusion
  13.7 0.1 subtract_convert_fusion.1
  13.8 0.1 pad_maximum_fusion.1
  13.9 0.1 convert_element_type.110
  14.0 0.1 slice_bitcast_fusion.4
  14.1 0.1 fusion.57
  14.2 2.5 %fusion.11 = f32[16,4,512]{2,1,0:T(4,128)S(1)} fusion(bf16[16,4,64]{2,1,0:T(4,128)(2,1)S(1)} %get-tuple-element.12, bf16[16,1,512,256]{3,2,1,0:T(8,128)(2,1)} %param.22), kind=kOutput, calls=%fused_computation.13 | convolution fusion | flops 4227072 | bytes 2236416 | tf_op jit(solution)/shard_map/bgjd,bgkd->bgjk/dot_general | solution.py:55
  16.7 0.1 fusion.61
  16.9 0.2 fusion.78
  17.1 0.1 fusion.63
  17.2 2.3 %select_reduce_fusion.1 = (f32[16,4]{1,0:T(8,128)S(1)}, f32[16,4]{1,0:T(8,128)S(1)}, f32[16,4,512]{2,1,0:T(4,128)S(1)}) fusion(pred[16,512]{1,0:T(8,128)(4,1)S(1)} %iota_compare_fusion, f32[16,4,512]{2,1,0:T(4,128)S(1)} %fusion.11, bf16[16,4,64]{2,1,0:T(4,128)(2,1)S(1)} %get-tuple-element.13, bf16[16,1,512,256]{3,2,1,0:T(8,128)(2,1)} %param.22), kind=kOutput, calls=%fused_computation.37 | convolution fusion | flops 4358016 | bytes 2376192 | tf_op jit(solution)/shard_map/bgjd,bgkd->bgjk/dot_general | solution.py:46
  19.6 0.3 fusion.36
  20.0 0.6 multiply_reduce_fusion.3
  20.6 0.1 broadcast_multiply_fusion
  20.7 6.2 %all_gather.6 = bf16[16,2048]{1,0:T(8,128)(2,1)S(1)} all-gather(bf16[16,512]{1,0:T(8,128)(2,1)S(1)} %fusion.47), channel_id=1, replica_groups=mesh['ep'=8,'tp'=4] {'tp'}, dimensions={1}, use_global_device_ids=true | all-gather | bytes 81920 | tf_op jit(solution)/shard_map/all_gather | solution.py:148
  26.9 2.0 %fusion.16 = bf16[16,512]{1,0:T(8,128)(2,1)S(1)} fusion(bf16[16,2048]{1,0:T(8,128)(2,1)S(1)} %all_gather.6, bf16[2048,512]{1,0:T(8,128)(2,1)} %param.29, f32[16,2048]{1,0:T(8,128)S(1)} %convert_element_type.107, s32[]{:T(128)S(6)} %select_n.47), kind=kOutput, calls=%fused_computation.19 | convolution fusion | flops 33570816 | bytes 2211844 | tf_op jit(solution)/shard_map/dot_general | solution.py:149
  29.0 5.5 %all_gather.7 = bf16[16,2048]{1,0:T(8,128)(2,1)S(1)} all-gather(bf16[16,512]{1,0:T(8,128)(2,1)S(1)} %fusion.16), channel_id=1, replica_groups=mesh['ep'=8,'tp'=4] {'tp'}, dimensions={1}, use_global_device_ids=true | all-gather | bytes 81920 | tf_op jit(solution)/shard_map/all_gather | solution.py:152
  34.5 0.1 fusion.23
  34.6 0.2 multiply_reduce_fusion
  34.9 1.7 %collective-permute-start = (bf16[4,2048]{1,0:T(4,128)(2,1)S(1)}, bf16[4,2048]{1,0:T(4,128)(2,1)S(1)}, u32[]{:S(2)}, u32[]{:S(2)}) collective-permute-start(bf16[4,2048]{1,0:T(4,128)(2,1)S(1)} %constant_dynamic-slice_fusion), channel_id=1, source_target_pairs={{0,4},{4,8},{8,12},{12,16},{16,20},{20,24},{24,28},{28,0},{1,5},{5... | collective-permute-start | bytes 49160 | tf_op jit(solution)/shard_map/ppermute | solution.py:191
  36.6 0.1 copy.69
  36.7 0.1 eq.31
  36.8 0.1 fusion.59
  36.9 4.5 %collective-permute-done = bf16[4,2048]{1,0:T(4,128)(2,1)S(1)} collective-permute-done((bf16[4,2048]{1,0:T(4,128)(2,1)S(1)}, bf16[4,2048]{1,0:T(4,128)(2,1)S(1)}, u32[]{:S(2)}, u32[]{:S(2)}) %collective-permute-start) | collective-permute-done | bytes 16416 | tf_op jit(solution)/shard_map/ppermute | solution.py:191
  41.4 0.2 select_reduce_fusion.2
  41.5 0.1 reduce_sum.79
  41.6 0.1 copy.70
  41.7 6.1 %collective-permute-done.1 = bf16[4,2048]{1,0:T(4,128)(2,1)S(1)} collective-permute-done((bf16[4,2048]{1,0:T(4,128)(2,1)S(1)}, bf16[4,2048]{1,0:T(4,128)(2,1)S(1)}, u32[]{:S(2)}, u32[]{:S(2)}) %collective-permute-start.1) | collective-permute-done | bytes 16416 | tf_op jit(solution)/shard_map/ppermute | solution.py:191
  47.8 6.4 %collective-permute-done.2 = bf16[4,2048]{1,0:T(4,128)(2,1)S(1)} collective-permute-done((bf16[4,2048]{1,0:T(4,128)(2,1)S(1)}, bf16[4,2048]{1,0:T(4,128)(2,1)S(1)}, u32[]{:S(2)}, u32[]{:S(2)}) %collective-permute-start.2) | collective-permute-done | bytes 16416 | tf_op jit(solution)/shard_map/ppermute | solution.py:191
  54.2 0.1 fusion.60
  54.3 6.4 %collective-permute-done.3 = bf16[4,2048]{1,0:T(4,128)(2,1)S(1)} collective-permute-done((bf16[4,2048]{1,0:T(4,128)(2,1)S(1)}, bf16[4,2048]{1,0:T(4,128)(2,1)S(1)}, u32[]{:S(2)}, u32[]{:S(2)}) %collective-permute-start.3) | collective-permute-done | bytes 16416 | tf_op jit(solution)/shard_map/ppermute | solution.py:191
  60.7 1.0 fusion
  61.6 6.0 %all-to-all-start = ((bf16[8,8,2048]{2,1,0:T(8,128)(2,1)}), bf16[8,8,2048]{2,1,0:T(8,128)(2,1)S(1)}, u32[]{:S(2)}, u32[]{:S(2)}) async-start(bf16[8,8,2048]{2,1,0:T(8,128)(2,1)} %fusion), calls=%async_computation | async-start | bytes 524288 | tf_op jit(solution)/shard_map/all_to_all | solution.py:169
  67.7 2.0 %collective-permute-start.5 = (bf16[4,2048]{1,0:T(4,128)(2,1)S(1)}, bf16[4,2048]{1,0:T(4,128)(2,1)S(1)}, u32[]{:S(2)}, u32[]{:S(2)}) collective-permute-start(bf16[4,2048]{1,0:T(4,128)(2,1)S(1)} %collective-permute-done.4), channel_id=1, source_target_pairs={{0,4},{4,8},{8,12},{12,16},{16,20},{20,24},{24,28},{28,0},{1,5},{5... | collective-permute-start | bytes 49160 | tf_op jit(solution)/shard_map/ppermute | solution.py:191
  69.7 6.8 %collective-permute-done.5 = bf16[4,2048]{1,0:T(4,128)(2,1)S(1)} collective-permute-done((bf16[4,2048]{1,0:T(4,128)(2,1)S(1)}, bf16[4,2048]{1,0:T(4,128)(2,1)S(1)}, u32[]{:S(2)}, u32[]{:S(2)}) %collective-permute-start.5) | collective-permute-done | bytes 16416 | tf_op jit(solution)/shard_map/ppermute | solution.py:191
  76.6 0.6 pad_maximum_fusion.2
  77.2 0.1 copy.71
  77.2 0.1 reshape.355
  77.4 0.6 dynamic-slice
  78.6 4.4 %collective-permute-done.6 = bf16[4,2048]{1,0:T(4,128)(2,1)S(1)} collective-permute-done((bf16[4,2048]{1,0:T(4,128)(2,1)S(1)}, bf16[4,2048]{1,0:T(4,128)(2,1)S(1)}, u32[]{:S(2)}, u32[]{:S(2)}) %collective-permute-start.6) | collective-permute-done | bytes 16416 | tf_op jit(solution)/shard_map/ppermute | solution.py:191
  83.0 0.3 concatenate.34
  83.3 3.0 %fusion.29 = f32[32,1024]{1,0:T(8,128)S(1)} fusion(bf16[2048,1024]{1,0:T(8,128)(2,1)} %param.36, bf16[64,2048]{1,0:T(8,128)(2,1)S(1)} %concatenate.34, s32[]{:T(128)S(6)} %select_n.57), kind=kOutput, calls=%fused_computation.43 | convolution fusion | flops 134217728 | bytes 4456452 | tf_op jit(solution)/shard_map/dot_general | solution.py:195
  86.3 1.3 convolution_bitcast_fusion.1
  87.6 2.1 %convolution_convert_fusion = bf16[8,8,2048]{2,1,0:T(8,128)(2,1)} fusion(bf16[8,8,2048]{2,1,0:T(8,128)(2,1)S(1)} %all-to-all-done, bf16[1,128,2048]{2,1,0:T(8,128)(2,1)S(1)} %copy-done.3, bf16[1,2048,128]{2,1,0:T(8,128)(2,1)} %param.34, f32[8,1,8,128]{3,2,0,1:T(8,128)S(1)} %convolution_bitcast_fusion.1), kind=kOutput, calls=%fused_computation.1 | convolution fusion | flops 67289088 | bytes 1605632 | tf_op jit(solution)/shard_map/sjcf,jfd->sjcd/dot_general | solution.py:175
  89.7 5.1 %fusion.34 = f32[32,2048]{1,0:T(8,128)S(1)} fusion(bf16[1024,2048]{1,0:T(8,128)(2,1)} %param.38, f32[32,1024]{1,0:T(8,128)S(1)} %fusion.29, bf16[2048,1024]{1,0:T(8,128)(2,1)} %param.37, bf16[64,2048]{1,0:T(8,128)(2,1)S(1)} %concatenate.34, s32[]{:T(128)S(6)} %select_n.57), kind=kOutput, calls=%fused_computation.45 | convolution fusion | flops 268632064 | bytes 8912900 | tf_op jit(solution)/shard_map/dot_general | solution.py:199
  94.8 36.2 %all-reduce.2 = bf16[32,2048]{1,0:T(8,128)(2,1)S(1)} all-reduce(f32[32,2048]{1,0:T(8,128)S(1)} %fusion.34), channel_id=3, replica_groups=mesh['ep'=8,'tp'=4] {'ep'}, use_global_device_ids=true, to_apply=%region_13.14.clone | all-reduce | flops 65536 | bytes 393216
  131.0 0.6 dynamic-slice_convert_fusion
  131.6 3.3 %all-to-all-start.2 = ((bf16[4,4,512]{2,0,1:T(4,128)(2,1)}), bf16[4,4,512]{2,0,1:T(4,128)(2,1)S(1)}, u32[]{:S(2)}, u32[]{:S(2)}) async-start(bf16[4,4,512]{2,0,1:T(4,128)(2,1)} %bitcast.34), calls=%async_computation.3 | async-start | bytes 32768 | tf_op jit(solution)/shard_map/all_to_all | solution.py:204
  134.9 0.1 copy.68
  135.0 3.7 %all-to-all-done.2 = bf16[4,4,512]{2,0,1:T(4,128)(2,1)S(1)} async-done(((bf16[4,4,512]{2,0,1:T(4,128)(2,1)}), bf16[4,4,512]{2,0,1:T(4,128)(2,1)S(1)}, u32[]{:S(2)}, u32[]{:S(2)}) %all-to-all-start.2) | async-done | bytes 16416 | tf_op jit(solution)/shard_map/all_to_all | solution.py:204
  138.7 3.8 %all-to-all-start.1 = ((bf16[8,8,512]{2,1,0:T(8,128)(2,1)}), bf16[8,8,512]{2,1,0:T(8,128)(2,1)S(1)}, u32[]{:S(2)}, u32[]{:S(2)}) async-start(bf16[8,8,512]{2,1,0:T(8,128)(2,1)} %reduce-scatter.2.cloned.1.call-done), calls=%async_computation.2 | async-start | bytes 131072 | tf_op jit(solution)/shard_map/all_to_all | solution.py:182
  142.6 6.9 %all-to-all-done.1 = bf16[8,8,512]{2,1,0:T(8,128)(2,1)S(1)} async-done(((bf16[8,8,512]{2,1,0:T(8,128)(2,1)}), bf16[8,8,512]{2,1,0:T(8,128)(2,1)S(1)}, u32[]{:S(2)}, u32[]{:S(2)}) %all-to-all-start.1) | async-done | bytes 65568 | tf_op jit(solution)/shard_map/all_to_all | solution.py:182
  149.4 0.6 gather_fusion
  150.1 0.1 multiply_reduce_fusion.2
  150.3 0.7 add_convert_fusion.1
  (53 shorter events, 0.4 us)
Async XLA Ops:
  7.2 3.4 %copy-start = (bf16[2048,512]{1,0:T(8,128)(2,1)S(1)}, bf16[2048,512]{1,0:T(8,128)(2,1)}, u32[]{:S(2)}) copy-start(bf16[2048,512]{1,0:T(8,128)(2,1)} %param.24) | copy-start | bytes 6291460
  7.2 9.6 %copy-start.1 = (bf16[16,2048]{1,0:T(8,128)(2,1)S(1)}, bf16[16,2048]{1,0:T(8,128)(2,1)}, u32[]{:S(2)}) copy-start(bf16[16,2048]{1,0:T(8,128)(2,1)} %param.20) | copy-start | bytes 196612
  7.2 9.6 %copy-start.5 = (f32[2048]{0:T(1024)S(1)}, f32[2048]{0:T(1024)}, u32[]{:S(2)}) copy-start(f32[2048]{0:T(1024)} %param.23) | copy-start | bytes 24580
  7.2 9.6 %copy-start.4 = (bf16[2048,128]{1,0:T(8,128)(2,1)S(1)}, bf16[2048,128]{1,0:T(8,128)(2,1)}, u32[]{:S(2)}) copy-start(bf16[2048,128]{1,0:T(8,128)(2,1)} %param.26) | copy-start | bytes 1572868
  10.6 9.3 %copy-start.10 = (f32[4]{0:T(128)S(1)}, f32[4]{0:T(128)}, u32[]{:S(2)}) copy-start(f32[4]{0:T(128)} %param.27) | copy-start | bytes 52
  14.0 6.0 %copy-start.2 = (bf16[16,1,512,256]{3,2,1,0:T(8,128)(2,1)S(1)}, bf16[16,1,512,256]{3,2,1,0:T(8,128)(2,1)}, u32[]{:S(2)}) copy-start(bf16[16,1,512,256]{3,2,1,0:T(8,128)(2,1)} %param.22) | copy-start | bytes 12582916
  16.9 3.7 %copy-start.11 = (f32[128]{0:T(128)S(1)}, f32[128]{0:T(128)}, u32[]{:S(2)}) copy-start(f32[128]{0:T(128)} %param.28) | copy-start | bytes 1540
  19.6 15.0 %copy-start.6 = (f32[2048]{0:T(1024)S(1)}, f32[2048]{0:T(1024)}, u32[]{:S(2)}) copy-start(f32[2048]{0:T(1024)} %param.39) | copy-start | bytes 24580
  19.6 15.0 %copy-start.7 = (f32[2048]{0:T(1024)S(1)}, f32[2048]{0:T(1024)}, u32[]{:S(2)}) copy-start(f32[2048]{0:T(1024)} %param.30) | copy-start | bytes 24580
  19.6 17.0 %copy-start.8 = (s32[16,2]{0,1:T(2,128)S(1)}, s32[16,2]{0,1:T(2,128)}, u32[]{:S(2)}) copy-start(s32[16,2]{0,1:T(2,128)} %param.31) | copy-start | bytes 388
  20.0 57.4 %copy-start.12 = (u32[32]{0:T(128)S(1)}, u32[32]{0:T(128)}, u32[]{:S(2)}) copy-start(u32[32]{0:T(128)} %constant.87) | copy-start | bytes 388
  26.9 60.6 %copy-start.3 = (bf16[1,128,2048]{2,1,0:T(8,128)(2,1)S(1)}, bf16[1,128,2048]{2,1,0:T(8,128)(2,1)}, u32[]{:S(2)}) copy-start(bf16[1,128,2048]{2,1,0:T(8,128)(2,1)} %param.35) | copy-start | bytes 1572868
  34.9 6.5 %collective-permute-start = (bf16[4,2048]{1,0:T(4,128)(2,1)S(1)}, bf16[4,2048]{1,0:T(4,128)(2,1)S(1)}, u32[]{:S(2)}, u32[]{:S(2)}) collective-permute-start(bf16[4,2048]{1,0:T(4,128)(2,1)S(1)} %constant_dynamic-slice_fusion), channel_id=1, source_target_pairs={{0,4},{4,8},{8,12},{12,16},{16,20},{20,24},{24,28},{28,0},{1,5},{5... | collective-permute-start | bytes 49160 | tf_op jit(solution)/shard_map/ppermute | solution.py:191
  41.4 6.4 %collective-permute-start.1 = (bf16[4,2048]{1,0:T(4,128)(2,1)S(1)}, bf16[4,2048]{1,0:T(4,128)(2,1)S(1)}, u32[]{:S(2)}, u32[]{:S(2)}) collective-permute-start(bf16[4,2048]{1,0:T(4,128)(2,1)S(1)} %collective-permute-done), channel_id=1, source_target_pairs={{0,4},{4,8},{8,12},{12,16},{16,20},{20,24},{24,28},{28,0},{1,5},{5... | collective-permute-start | bytes 49160 | tf_op jit(solution)/shard_map/ppermute | solution.py:191
  47.8 6.4 %collective-permute-start.2 = (bf16[4,2048]{1,0:T(4,128)(2,1)S(1)}, bf16[4,2048]{1,0:T(4,128)(2,1)S(1)}, u32[]{:S(2)}, u32[]{:S(2)}) collective-permute-start(bf16[4,2048]{1,0:T(4,128)(2,1)S(1)} %collective-permute-done.1), channel_id=1, source_target_pairs={{0,4},{4,8},{8,12},{12,16},{16,20},{20,24},{24,28},{28,0},{1,5},{5... | collective-permute-start | bytes 49160 | tf_op jit(solution)/shard_map/ppermute | solution.py:191
  54.2 6.4 %collective-permute-start.3 = (bf16[4,2048]{1,0:T(4,128)(2,1)S(1)}, bf16[4,2048]{1,0:T(4,128)(2,1)S(1)}, u32[]{:S(2)}, u32[]{:S(2)}) collective-permute-start(bf16[4,2048]{1,0:T(4,128)(2,1)S(1)} %collective-permute-done.2), channel_id=1, source_target_pairs={{0,4},{4,8},{8,12},{12,16},{16,20},{20,24},{24,28},{28,0},{1,5},{5... | collective-permute-start | bytes 49160 | tf_op jit(solution)/shard_map/ppermute | solution.py:191
  60.7 7.0 %collective-permute-start.4 = (bf16[4,2048]{1,0:T(4,128)(2,1)S(1)}, bf16[4,2048]{1,0:T(4,128)(2,1)S(1)}, u32[]{:S(2)}, u32[]{:S(2)}) collective-permute-start(bf16[4,2048]{1,0:T(4,128)(2,1)S(1)} %collective-permute-done.3), channel_id=1, source_target_pairs={{0,4},{4,8},{8,12},{12,16},{16,20},{20,24},{24,28},{28,0},{1,5},{5... | collective-permute-start | bytes 49160 | tf_op jit(solution)/shard_map/ppermute | solution.py:191
  61.6 24.6 %all-to-all-start = ((bf16[8,8,2048]{2,1,0:T(8,128)(2,1)}), bf16[8,8,2048]{2,1,0:T(8,128)(2,1)S(1)}, u32[]{:S(2)}, u32[]{:S(2)}) async-start(bf16[8,8,2048]{2,1,0:T(8,128)(2,1)} %fusion), calls=%async_computation | async-start | bytes 524288 | tf_op jit(solution)/shard_map/all_to_all | solution.py:169
  67.6 71.1 %reduce-scatter.2.cloned.1.call-start = ((), (), s32[]{:S(2)}) async-start(), calls=%async_computation.4 | async-start | bytes 327680 | tf_op jit(solution)/shard_map/reduce_scatter | solution.py:179
  67.7 8.9 %collective-permute-start.5 = (bf16[4,2048]{1,0:T(4,128)(2,1)S(1)}, bf16[4,2048]{1,0:T(4,128)(2,1)S(1)}, u32[]{:S(2)}, u32[]{:S(2)}) collective-permute-start(bf16[4,2048]{1,0:T(4,128)(2,1)S(1)} %collective-permute-done.4), channel_id=1, source_target_pairs={{0,4},{4,8},{8,12},{12,16},{16,20},{20,24},{24,28},{28,0},{1,5},{5... | collective-permute-start | bytes 49160 | tf_op jit(solution)/shard_map/ppermute | solution.py:191
  76.5 6.4 %collective-permute-start.6 = (bf16[4,2048]{1,0:T(4,128)(2,1)S(1)}, bf16[4,2048]{1,0:T(4,128)(2,1)S(1)}, u32[]{:S(2)}, u32[]{:S(2)}) collective-permute-start(bf16[4,2048]{1,0:T(4,128)(2,1)S(1)} %collective-permute-done.5), channel_id=1, source_target_pairs={{0,4},{4,8},{8,12},{12,16},{16,20},{20,24},{24,28},{28,0},{1,5},{5... | collective-permute-start | bytes 49160 | tf_op jit(solution)/shard_map/ppermute | solution.py:191
  89.7 45.2 %copy-start.9 = (f32[16,2]{0,1:T(2,128)S(1)}, f32[16,2]{0,1:T(2,128)}, u32[]{:S(2)}) copy-start(f32[16,2]{0,1:T(2,128)} %param.32) | copy-start | bytes 388
  131.6 7.1 %all-to-all-start.2 = ((bf16[4,4,512]{2,0,1:T(4,128)(2,1)}), bf16[4,4,512]{2,0,1:T(4,128)(2,1)S(1)}, u32[]{:S(2)}, u32[]{:S(2)}) async-start(bf16[4,4,512]{2,0,1:T(4,128)(2,1)} %bitcast.34), calls=%async_computation.3 | async-start | bytes 32768 | tf_op jit(solution)/shard_map/all_to_all | solution.py:204
  138.7 10.7 %all-to-all-start.1 = ((bf16[8,8,512]{2,1,0:T(8,128)(2,1)}), bf16[8,8,512]{2,1,0:T(8,128)(2,1)S(1)}, u32[]{:S(2)}, u32[]{:S(2)}) async-start(bf16[8,8,512]{2,1,0:T(8,128)(2,1)} %reduce-scatter.2.cloned.1.call-done), calls=%async_computation.2 | async-start | bytes 131072 | tf_op jit(solution)/shard_map/all_to_all | solution.py:182
Sparse Core Ops, SparseCore 0:
  89.8 17.5 reduce-scatter.1
